TPU v7x, 32 devices: a whole 2x2x4 slice. The times are simulated.
32 devices in a mesh: sp: 16 (over z, y, x), tp: 2 (over core).
Axes of the slice: x: 2, y: 2, z: 4, core: 2. Of those that a mesh axis runs over, the one named last changes fastest.
Arguments:
- stream_in: bfloat16 [2048, 2048], P(('sp', 'tp')), may hold values from -6 to 6
- query_compressed: bfloat16 [2048, 512], P('sp'), may hold values from -6 to 6
- keyvalue_compressed: bfloat16 [2048, 256], P('sp'), may hold values from -6 to 6
- rope_key: bfloat16 [2048, 64], P('sp'), may hold values from -153 to 153
- query_norm_gain: float32 [512], replicated, may hold values from 0.1 to 1.9
- keyvalue_norm_gain: float32 [256], replicated, may hold values from 0.1 to 1.9
- query_up_weight: bfloat16 [512, 3072], replicated, may hold values from -0.625 to 0.625
- keyvalue_up_weight: bfloat16 [256, 4096], replicated, may hold values from -0.375 to 0.375
- out_proj: bfloat16 [2048, 2048], replicated, may hold values from -0.5 to 0.5
- ffn_gain: float32 [2048], replicated, may hold values from 0.1 to 1.9
- expert_ids: int32 [2048, 4], P(('sp', 'tp')), may hold values from 0 to 15, all different within a row; in each aligned block of 64 rows (0 to 63, 64 to 127, ...) at most 32 rows name the same one
- expert_weights: float32 [2048, 4], P(('sp', 'tp')), may hold values from 0.1 to 1
- expert_gate: bfloat16 [16, 2048, 512], P('sp', None, 'tp'), may hold values from -0.125 to 0.125
- expert_up: bfloat16 [16, 2048, 512], P('sp', None, 'tp'), may hold values from -0.125 to 0.125
- expert_down: bfloat16 [16, 512, 2048], P('sp', 'tp'), may hold values from -0.25 to 0.25
- shared_gate: bfloat16 [2048, 512], replicated, may hold values from -0.125 to 0.125
- shared_up: bfloat16 [2048, 512], replicated, may hold values from -0.125 to 0.125
- shared_down: bfloat16 [512, 2048], replicated, may hold values from -0.25 to 0.25
Outputs:
- layer_out: bfloat16 [2048, 2048], P(('sp', 'tp'))
Inputs may be any that keep to these rules, and one draw needn't show every extreme that they name: `expert_ids`: each row names 4 different experts. Among the rows of one device (aligned blocks of 64 rows in token order) no expert is named by more than 32 rows, a bound that some block reaches of some device.
All inputs are finite; a program needn't handle non-finite values.
Results may differ from a plain program's by a relative error of at most 0.02.
The roundings to bfloat16 on the way count: a program that leaves them out, or rounds other values in their place, can miss the bound.
Values may be sent and summed in bfloat16 or wider, within the bound.
A program may use at most 128 MiB of HBM per device.

v0:
```python
import jax
import jax.numpy as jnp
from jax import lax
from jax.sharding import PartitionSpec as P

KEY_PLAIN_WIDTH = 128
ROTARY_WIDTH = 64
VALUE_HEAD_WIDTH = 128
epsilon = 1e-06
routed_scale = 2.5
theta_base = 10000.0


def rms_scale(values, scales):
    widened = values.astype(jnp.float32)
    inverse = lax.rsqrt(jnp.mean(widened * widened, axis=-1, keepdims=True) + epsilon)
    return widened * inverse * scales


def turn_tables(positions, rot_width):
    half_width = rot_width // 2
    frequency = theta_base ** (-(jnp.arange(half_width, dtype=jnp.float32) * 2.0) / rot_width)
    angles = positions.astype(jnp.float32)[:, None] * frequency[None, :]
    return (jnp.cos(angles), jnp.sin(angles))


def turn(values, cos_part, sine_part):
    lower_half, upper_half = jnp.split(values, 2, axis=-1)
    return jnp.concatenate(
        [
            lower_half * cos_part - upper_half * sine_part,
            upper_half * cos_part + lower_half * sine_part,
        ],
        axis=-1,
    )


def key_span(piece_rows):
    for candidate in (1024, 512, 256, 128):
        return candidate
    return piece_rows


def expand_keys(lat_block, rot_block, key_pos, keyvalue_norm_gain, keyval_cols, head_count):
    keyval_normed = rms_scale(lat_block, keyvalue_norm_gain).astype(jnp.bfloat16)
    keyvals = jnp.dot(keyval_normed, keyval_cols, preferred_element_type=jnp.float32).astype(
        jnp.bfloat16
    )
    keyvals = keyvals.reshape(lat_block.shape[0], head_count, KEY_PLAIN_WIDTH + VALUE_HEAD_WIDTH)
    cos_part, sine_part = turn_tables(key_pos, rot_block.shape[-1])
    shared_rot = turn(rot_block.astype(jnp.float32), cos_part, sine_part).astype(jnp.bfloat16)
    return (keyvals[:, :, :KEY_PLAIN_WIDTH], keyvals[:, :, KEY_PLAIN_WIDTH:], shared_rot)


def absorb(carried, queries, key_part, value_part, shared_rot):
    run_max, run_sum, run_acc = carried
    scores = jnp.einsum(
        "qhd,khd->qhk",
        queries[:, :, :KEY_PLAIN_WIDTH],
        key_part,
        preferred_element_type=jnp.float32,
    )
    scores = scores + jnp.einsum(
        "qhr,kr->qhk",
        queries[:, :, KEY_PLAIN_WIDTH:],
        shared_rot,
        preferred_element_type=jnp.float32,
    )
    new_max = jnp.maximum(run_max, jnp.max(scores, axis=-1))
    factor = jnp.exp(run_max - new_max)
    weights = jnp.exp(scores - new_max[:, :, None])
    new_sum = run_sum * factor + jnp.sum(weights, axis=-1)
    new_acc = run_acc * factor[:, :, None] + jnp.einsum(
        "qhk,khd->qhd", weights.astype(jnp.bfloat16), value_part, preferred_element_type=jnp.float32
    )
    return (new_max, new_sum, new_acc)


def attend_all(
    queries, lat_shard, rot_shard, keyvalue_norm_gain, keyval_cols, head_count, place_rows
):
    query_rows = queries.shape[0]
    initial = (
        jnp.full((query_rows, head_count), -jnp.inf, jnp.float32),
        jnp.zeros((query_rows, head_count), jnp.float32),
        jnp.zeros((query_rows, head_count, VALUE_HEAD_WIDTH), jnp.float32),
    )
    lat_piece = lax.all_gather(lat_shard, "sp", axis=0, tiled=True)
    rot_piece = lax.all_gather(rot_shard, "sp", axis=0, tiled=True)
    span_rows = key_span(lat_piece.shape[0])
    block_total = lat_piece.shape[0] // span_rows

    def one_block(inner_carried, block_index):
        lat_block = lax.dynamic_slice_in_dim(lat_piece, block_index * span_rows, span_rows, 0)
        rot_block = lax.dynamic_slice_in_dim(rot_piece, block_index * span_rows, span_rows, 0)
        key_pos = place_rows(block_index * span_rows + jnp.arange(span_rows, dtype=jnp.int32))
        key_part, value_part, shared_rot = expand_keys(
            lat_block, rot_block, key_pos, keyvalue_norm_gain, keyval_cols, head_count
        )
        return (absorb(inner_carried, queries, key_part, value_part, shared_rot), None)

    result, _ = lax.scan(one_block, initial, jnp.arange(block_total, dtype=jnp.int32))
    return result


def shards(
    stream_in,
    query_compressed,
    keyvalue_compressed,
    rope_key,
    query_norm_gain,
    keyvalue_norm_gain,
    query_up_weight,
    keyvalue_up_weight,
    out_proj,
    ffn_gain,
    expert_ids,
    expert_weights,
    expert_gate,
    expert_up,
    expert_down,
    shared_gate,
    shared_up,
    shared_down,
):
    full_gate, full_up, full_down = (
        lax.all_gather(expert_gate, "tp", axis=2, tiled=True),
        lax.all_gather(expert_up, "tp", axis=2, tiled=True),
        lax.all_gather(expert_down, "tp", axis=1, tiled=True),
    )
    tok_rows = query_compressed.shape[0]
    head_width = KEY_PLAIN_WIDTH + ROTARY_WIDTH
    pair_width = KEY_PLAIN_WIDTH + VALUE_HEAD_WIDTH
    all_heads = query_up_weight.shape[1] // head_width
    sp_index = lax.axis_index("sp")
    tp_index = lax.axis_index("tp")
    own_pos = sp_index * tok_rows + jnp.arange(tok_rows, dtype=jnp.int32)
    query_normed = rms_scale(query_compressed, query_norm_gain).astype(jnp.bfloat16)
    local_heads = all_heads // 2
    query_cols = lax.dynamic_slice_in_dim(
        query_up_weight, tp_index * local_heads * head_width, local_heads * head_width, 1
    )
    keyval_cols = lax.dynamic_slice_in_dim(
        keyvalue_up_weight, tp_index * local_heads * pair_width, local_heads * pair_width, 1
    )
    raw_query = jnp.dot(
        query_normed, query_cols, preferred_element_type=jnp.float32
    ) * head_width ** (-0.5)
    raw_query = raw_query.reshape(tok_rows, local_heads, head_width)
    cos_part, sine_part = turn_tables(own_pos, ROTARY_WIDTH)
    turned = turn(raw_query[:, :, KEY_PLAIN_WIDTH:], cos_part[:, None, :], sine_part[:, None, :])
    queries = jnp.concatenate([raw_query[:, :, :KEY_PLAIN_WIDTH], turned], axis=-1).astype(
        jnp.bfloat16
    )

    def place_whole(whole_rows):
        return whole_rows

    run_max, run_sum, run_acc = attend_all(
        queries,
        keyvalue_compressed,
        rope_key,
        keyvalue_norm_gain,
        keyval_cols,
        local_heads,
        place_whole,
    )
    local_out = (
        (run_acc / run_sum[:, :, None])
        .astype(jnp.bfloat16)
        .reshape(tok_rows, local_heads * VALUE_HEAD_WIDTH)
    )
    attended = lax.all_to_all(local_out, "tp", split_axis=0, concat_axis=1, tiled=True)
    projected = jnp.dot(attended, out_proj, preferred_element_type=jnp.float32)
    stream = (stream_in.astype(jnp.float32) + projected).astype(jnp.bfloat16)
    normed = rms_scale(stream, ffn_gain).astype(jnp.bfloat16)
    shares = (
        routed_scale * expert_weights / jnp.sum(expert_weights, axis=-1, keepdims=True)
    ).astype(jnp.bfloat16)
    moe_rows = stream_in.shape[0]
    top_count = expert_ids.shape[1]
    sp_count = lax.axis_size("sp")
    local_experts = expert_gate.shape[0]
    expert_count = local_experts * sp_count
    capacity = 2 * moe_rows * top_count // expert_count
    flat_ids = expert_ids.reshape(-1)
    hot_ids = (flat_ids[:, None] == jnp.arange(expert_count, dtype=jnp.int32)[None, :]).astype(
        jnp.int32
    )
    rank_ids = jnp.sum((jnp.cumsum(hot_ids, axis=0) - hot_ids) * hot_ids, axis=1)
    slot_ids = flat_ids * capacity + rank_ids
    hot_slots = (
        slot_ids[:, None] == jnp.arange(expert_count * capacity, dtype=jnp.int32)[None, :]
    ).reshape(moe_rows, top_count, expert_count * capacity)
    sender_map = jnp.any(hot_slots, axis=1).astype(jnp.bfloat16)
    combine = jnp.sum(jnp.where(hot_slots, shares[:, :, None], jnp.zeros((), jnp.bfloat16)), axis=1)
    outgoing = jnp.einsum(
        "ts,td->sd", sender_map, normed, preferred_element_type=jnp.float32
    ).astype(jnp.bfloat16)
    outgoing = outgoing.reshape(sp_count, local_experts, capacity, normed.shape[1])
    arrived = lax.all_to_all(outgoing, "sp", split_axis=0, concat_axis=0, tiled=True)
    gate_act = jnp.einsum("secd,edf->secf", arrived, full_gate, preferred_element_type=jnp.float32)
    up_act = jnp.einsum("secd,edf->secf", arrived, full_up, preferred_element_type=jnp.float32)
    inner_act = (jax.nn.silu(gate_act) * up_act).astype(jnp.bfloat16)
    half_hidden = inner_act.shape[-1] // 2
    first_half = jnp.einsum(
        "secf,efd->secd",
        inner_act[..., :half_hidden],
        full_down[:, :half_hidden],
        preferred_element_type=jnp.float32,
    ).astype(jnp.bfloat16)
    second_half = jnp.einsum(
        "secf,efd->secd",
        inner_act[..., half_hidden:],
        full_down[:, half_hidden:],
        preferred_element_type=jnp.float32,
    ).astype(jnp.bfloat16)
    summed = (first_half.astype(jnp.float32) + second_half.astype(jnp.float32)).astype(jnp.bfloat16)
    returned = lax.all_to_all(summed, "sp", split_axis=0, concat_axis=0, tiled=True)
    routed = jnp.dot(
        combine,
        returned.reshape(expert_count * capacity, normed.shape[1]),
        preferred_element_type=jnp.float32,
    )
    shared_inner = (
        jax.nn.silu(jnp.dot(normed, shared_gate, preferred_element_type=jnp.float32))
        * jnp.dot(normed, shared_up, preferred_element_type=jnp.float32)
    ).astype(jnp.bfloat16)
    shared_out = jnp.dot(shared_inner, shared_down, preferred_element_type=jnp.float32)
    return (stream.astype(jnp.float32) + routed + shared_out).astype(jnp.bfloat16)


def solution(mesh):
    in_specs = (
        P(("sp", "tp"), None),
        P("sp", None),
        P("sp", None),
        P("sp", None),
        P(),
        P(),
        P(),
        P(),
        P(),
        P(),
        P(("sp", "tp"), None),
        P(("sp", "tp"), None),
        P("sp", None, "tp"),
        P("sp", None, "tp"),
        P("sp", "tp", None),
        P(),
        P(),
        P(),
    )
    out_specs = P(("sp", "tp"), None)
    return jax.shard_map(shards, mesh=mesh, in_specs=in_specs, out_specs=out_specs, check_vma=False)
```

profile of v0, /device:TPU:12, one launch (start us, length us, event | category | flops | bytes accessed | tf_op | source)
XLA Modules:
  0.0 256.1 jit_solution(11174466686180340704)
XLA Ops:
  6.5 0.7 all-gather.5.cloned.1.call-update
  7.3 0.7 all-gather.7.cloned.1.call-update
  8.1 0.8 copy.82
  9.0 1.0 fusion.74
  10.1 2.2 convolution_multiply_fusion
  12.3 1.4 copy.78
  14.3 35.2 %all_gather.16 = bf16[2048,64]{0,1:T(8,128)(2,1)} all-gather(bf16[128,64]{0,1:T(8,128)(2,1)S(1)} %copy-done.13), channel_id=1, replica_groups=mesh['sp'=16,'tp'=2] {'sp'}, dimensions={0}, use_global_device_ids=true | all-gather | bytes 278528 | tf_op jit(solution)/shard_map/all_gather | solution.py:89
  50.5 0.7 fusion.72
  51.3 2.3 constant_dynamic-slice_fusion
  53.6 12.2 %all-gather.5.cloned.1.call-done = bf16[2048,256]{1,0:T(8,128)(2,1)} async-done(((bf16[128,256]{1,0:T(8,128)(2,1)}), bf16[2048,256]{1,0:T(8,128)(2,1)}) %all-gather.5.cloned.1.call-update) | async-done | bytes 1048592 | tf_op jit(solution)/shard_map/all_gather | solution.py:88
  65.8 45.4 %while.15 = (s32[]{:T(128)}, f32[128,8]{0,1:T(8,128)S(1)}, f32[128,8]{0,1:T(8,128)S(1)}, f32[128,8,128]{0,2,1:T(8,128)}, s32[2]{0:T(128)S(1)}, /*index=5*/bf16[2...) while((s32[]{:T(128)}, f32[128,8]{0,1:T(8,128)S(1)}, ...), condition=%wide.region_5.6_spmd.clone, body=%wide.region_1.5_spmd.clone.sunk | while | flops 1756078208 | bytes 72443560 | solution.py:102
  65.8 0.6 dynamic_slice.37
  67.1 1.3 fusion.130
  68.4 2.7 %convolution_convert_fusion.5 = bf16[1024,2048]{1,0:T(8,128)(2,1)S(1)} fusion(bf16[256,2048]{1,0:T(8,128)(2,1)} %get-tuple-element.279, f32[256]{0:T(256)S(1)} %get-tuple-element.278, f32[1024]{0:T(1024)S(1)} %add_rsqrt_fusion.4, bf16[2048,256]{1,0:T(8,128)(2,1)} %get-tuple-element.277, s32[]{:T(128)S(6)} %select_n.22), kind=kOutput, calls=%fused_computation.2.clone.1 | convolution fusion | flops 1076887552 | bytes 5772292 | tf_op jit(solution)/shard_map/while/body/eval_jaxpr/dot_general | solution.py:46
  71.1 1.5 copy.110
  72.8 2.7 %fusion.132 = f32[8,1024,128]{2,1,0:T(8,128)} fusion(bf16[1024,8,128]{2,1,0:T(8,128)(2,1)S(1)} %get-tuple-element.238, bf16[128,8,192]{2,0,1:T(8,128)(2,1)S(1)} %get-tuple-element.280), kind=kOutput, calls=%fused_computation.7.clone.1 | convolution fusion | flops 268435456 | bytes 6553600 | tf_op jit(solution)/shard_map/while/body/eval_jaxpr/qhd,khd->qhk/dot_general | solution.py:57
  75.5 0.9 dynamic-slice_convert_fusion.2
  76.5 1.2 fusion.129
  77.9 5.0 %fusion.133 = (f32[128,8]{0,1:T(8,128)S(1)}, f32[128,8,1024]{0,2,1:T(8,128)}) fusion(bf16[128,8,192]{0,2,1:T(8,128)(2,1)S(1)} %copy.109, bf16[1024,32]{0,1:T(8,128)(2,1)} %get-tuple-element.236, bf16[1024,32]{0,1:T(8,128)(2,1)} %get-tuple-element.237, f32[8,1024,128]{2,1,0:T(8,128)} %fusion.132), kind=kOutput, calls=%fused_computation.121.clone.1 | convolution fusion | flops 136576000 | bytes 8654848 | tf_op jit(solution)/shard_map/while/body/eval_jaxpr/qhr,kr->qhk/dot_general | solution.py:63
  83.0 2.9 %fusion.134 = f32[128,8]{0,1:T(8,128)S(1)} fusion(f32[128,8,1024]{0,2,1:T(8,128)} %get-tuple-element.240, f32[128,8]{0,1:T(8,128)S(1)} %select_maximum_fusion.2), kind=kLoop, calls=%fused_computation.4.clone.1 | loop fusion | flops 2096128 | bytes 4202496 | tf_op jit(solution)/shard_map/while/body/eval_jaxpr/reduce_sum | solution.py:72
  86.4 1.3 fusion.136
  87.7 0.8 copy-done.4
  89.8 1.3 fusion.130
  91.1 2.7 %convolution_convert_fusion.5 = bf16[1024,2048]{1,0:T(8,128)(2,1)S(1)} fusion(bf16[256,2048]{1,0:T(8,128)(2,1)} %get-tuple-element.279, f32[256]{0:T(256)S(1)} %get-tuple-element.278, f32[1024]{0:T(1024)S(1)} %add_rsqrt_fusion.4, bf16[2048,256]{1,0:T(8,128)(2,1)} %get-tuple-element.277, s32[]{:T(128)S(6)} %select_n.22), kind=kOutput, calls=%fused_computation.2.clone.1 | convolution fusion | flops 1076887552 | bytes 5772292 | tf_op jit(solution)/shard_map/while/body/eval_jaxpr/dot_general | solution.py:46
  93.8 1.5 copy.110
  95.5 2.7 %fusion.132 = f32[8,1024,128]{2,1,0:T(8,128)} fusion(bf16[1024,8,128]{2,1,0:T(8,128)(2,1)S(1)} %get-tuple-element.238, bf16[128,8,192]{2,0,1:T(8,128)(2,1)S(1)} %get-tuple-element.280), kind=kOutput, calls=%fused_computation.7.clone.1 | convolution fusion | flops 268435456 | bytes 6553600 | tf_op jit(solution)/shard_map/while/body/eval_jaxpr/qhd,khd->qhk/dot_general | solution.py:57
  98.2 0.9 dynamic-slice_convert_fusion.2
  99.2 1.2 fusion.129
  100.6 5.0 %fusion.133 = (f32[128,8]{0,1:T(8,128)S(1)}, f32[128,8,1024]{0,2,1:T(8,128)}) fusion(bf16[128,8,192]{0,2,1:T(8,128)(2,1)S(1)} %copy.109, bf16[1024,32]{0,1:T(8,128)(2,1)} %get-tuple-element.236, bf16[1024,32]{0,1:T(8,128)(2,1)} %get-tuple-element.237, f32[8,1024,128]{2,1,0:T(8,128)} %fusion.132), kind=kOutput, calls=%fused_computation.121.clone.1 | convolution fusion | flops 136576000 | bytes 8654848 | tf_op jit(solution)/shard_map/while/body/eval_jaxpr/qhr,kr->qhk/dot_general | solution.py:63
  105.6 2.9 %fusion.134 = f32[128,8]{0,1:T(8,128)S(1)} fusion(f32[128,8,1024]{0,2,1:T(8,128)} %get-tuple-element.240, f32[128,8]{0,1:T(8,128)S(1)} %select_maximum_fusion.2), kind=kLoop, calls=%fused_computation.4.clone.1 | loop fusion | flops 2096128 | bytes 4202496 | tf_op jit(solution)/shard_map/while/body/eval_jaxpr/reduce_sum | solution.py:72
  109.1 1.3 fusion.136
  110.4 0.8 copy-done.4
  111.2 1.1 divide_convert_fusion
  112.7 3.9 %all_to_all.29 = bf16[2,64,1024]{2,1,0:T(8,128)(2,1)S(1)} all-to-all(bf16[2,64,1024]{2,1,0:T(8,128)(2,1)S(1)} %all_to_all.20), channel_id=1, replica_groups=mesh['sp'=16,'tp'=2] {'tp'}, dimensions={0} | all-to-all | bytes 524288 | tf_op jit(solution)/shard_map/all_to_all | solution.py:173
  116.7 5.1 %multiply_reduce_fusion = (f32[64]{0:T(128)S(1)}, f32[64,2048]{1,0:T(8,128)S(1)}) fusion(bf16[64,2048]{1,0:T(8,128)(2,1)S(1)} %bitcast.138, bf16[2048,2048]{1,0:T(8,128)(2,1)} %param.28, bf16[64,2048]{1,0:T(8,128)(2,1)S(1)} %copy-done.8), kind=kOutput, calls=%fused_computation.75 | convolution fusion | flops 537657280 | bytes 9437440 | tf_op jit(solution)/shard_map/dot_general | solution.py:174
  121.9 2.1 convolution_convert_fusion.3
  124.1 5.9 %all-to-all-start.1 = ((bf16[16,1,32,2048]{3,2,1,0:T(8,128)(2,1)}), bf16[16,1,32,2048]{3,2,1,0:T(8,128)(2,1)S(1)}, u32[]{:S(2)}, u32[]{:S(2)}) async-start(bf16[16,1,32,2048]{3,2,1,0:T(8,128)(2,1)} %bitcast.4), calls=%async_computation.1 | async-start | bytes 4194304 | tf_op jit(solution)/shard_map/all_to_all | solution.py:201
  130.0 0.7 all-gather.9.cloned.1.call-update
  131.3 47.0 %all-to-all-done.1 = bf16[16,1,32,2048]{3,2,1,0:T(8,128)(2,1)S(1)} async-done(((bf16[16,1,32,2048]{3,2,1,0:T(8,128)(2,1)}), bf16[16,1,32,2048]{3,2,1,0:T(8,128)(2,1)S(1)}, u32[]{:S(2)}, u32[]{:S(2)}) %all-to-all-start.1) | async-done | bytes 2097184 | tf_op jit(solution)/shard_map/all_to_all | solution.py:201
  178.3 3.8 %fusion.51 = f32[16,1,32,512]{3,2,0,1:T(8,128)} fusion(bf16[1,2048,512]{2,1,0:T(8,128)(2,1)} %all-gather.7.cloned.1.call-done, bf16[16,1,32,2048]{3,2,1,0:T(8,128)(2,1)S(1)} %all-to-all-done.1), kind=kOutput, calls=%fused_computation.65 | convolution fusion | flops 1073741824 | bytes 5242880 | tf_op jit(solution)/shard_map/secd,edf->secf/dot_general | solution.py:202
  182.2 3.2 %fusion.66 = bf16[16,1,32,512]{3,2,0,1:T(8,128)(2,1)S(1)} fusion(bf16[1,2048,512]{2,1,0:T(8,128)(2,1)} %all-gather.9.cloned.1.call-done, bf16[16,1,32,2048]{3,2,1,0:T(8,128)(2,1)S(1)} %all-to-all-done.1, f32[16,1,32,512]{3,2,0,1:T(8,128)} %fusion.51), kind=kOutput, calls=%fused_computation.68 | convolution fusion | flops 1075314688 | bytes 5767168 | tf_op jit(solution)/shard_map/secd,edf->secf/dot_general | solution.py:203
  185.4 2.1 convolution_convert_fusion.1
  187.5 2.0 fusion.40
  189.5 5.2 %all-to-all-start.2 = ((bf16[16,1,32,2048]{3,2,1,0:T(8,128)(2,1)}), bf16[16,1,32,2048]{3,2,1,0:T(8,128)(2,1)}, u32[]{:S(2)}, u32[]{:S(2)}) async-start(bf16[16,1,32,2048]{3,2,1,0:T(8,128)(2,1)} %fusion.40), calls=%async_computation.2 | async-start | bytes 4194304 | tf_op jit(solution)/shard_map/all_to_all | solution.py:219
  194.8 0.8 fusion.77
  196.0 46.5 %all-to-all-done.2 = bf16[16,1,32,2048]{3,2,1,0:T(8,128)(2,1)} async-done(((bf16[16,1,32,2048]{3,2,1,0:T(8,128)(2,1)}), bf16[16,1,32,2048]{3,2,1,0:T(8,128)(2,1)}, u32[]{:S(2)}, u32[]{:S(2)}) %all-to-all-start.2) | async-done | bytes 2097184 | tf_op jit(solution)/shard_map/all_to_all | solution.py:219
  242.6 3.1 %convolution_add_fusion.1 = f32[64,2048]{1,0:T(8,128)} fusion(f32[64,2048]{1,0:T(8,128)} %copy-done.5, bf16[64,512]{1,0:T(8,128)(2,1)} %fusion.77, bf16[512,2048]{1,0:T(8,128)(2,1)} %bitcast.28), kind=kOutput, calls=%fused_computation.53 | convolution fusion | flops 134348800 | bytes 3211264 | tf_op jit(solution)/shard_map/dot_general | solution.py:220
  245.7 3.9 %fusion.43 = bf16[64,2048]{1,0:T(8,128)(2,1)} fusion(f32[64,2048]{1,0:T(8,128)} %convolution_add_fusion.1, bf16[512,2048]{1,0:T(8,128)(2,1)} %param.37, bf16[64,2048]{1,0:T(8,128)(2,1)S(1)} %multiply_convert_fusion, bf16[2048,512]{1,0:T(8,128)(2,1)} %param.36, f32[64,512]{1,0:T(8,128)S(1)} %fusion.96), kind=kOutput, calls=%fused_computation.57 | convolution fusion | flops 268894208 | bytes 5373952 | tf_op jit(solution)/shard_map/dot_general | solution.py:229
  (102 shorter events, 6.2 us)
Async XLA Ops:
  6.5 3.5 %copy-start = (bf16[512,3072]{1,0:T(8,128)(2,1)S(1)}, bf16[512,3072]{1,0:T(8,128)(2,1)}, u32[]{:S(2)}) copy-start(bf16[512,3072]{1,0:T(8,128)(2,1)} %param.26) | copy-start | bytes 9437188
  6.5 59.3 %all-gather.5.cloned.1.call-start = ((), (), s32[]{:S(2)}) async-start(), calls=%async_computation.3 | async-start | bytes 1114112 | tf_op jit(solution)/shard_map/all_gather | solution.py:88
  7.3 124.0 %all-gather.7.cloned.1.call-start = ((), (), s32[]{:S(2)}) async-start(), calls=%async_computation.4 | async-start | bytes 3145728 | tf_op jit(solution)/shard_map/all_gather | solution.py:127
  12.3 2.0 copy-start.13
  12.3 38.2 %copy-start.15 = (s32[64,4]{0,1:T(4,128)S(1)}, s32[64,4]{0,1:T(4,128)}, u32[]{:S(2)}) copy-start(s32[64,4]{0,1:T(4,128)} %param.30) | copy-start | bytes 3076
  14.0 51.8 %copy-start.10 = (f32[256]{0:T(256)S(1)}, f32[256]{0:T(256)}, u32[]{:S(2)}) copy-start(f32[256]{0:T(256)} %param.25) | copy-start | bytes 3076
  50.5 15.3 %copy-start.11 = (s32[64,4]{0,1:T(4,128)}, s32[64,4]{0,1:T(4,128)S(1)}, u32[]{:S(2)}) copy-start(s32[64,4]{0,1:T(4,128)S(1)} %multiply_add_fusion) | copy-start | bytes 3076
  65.8 5.2 %copy-start.17 = (s32[2]{0:T(128)}, s32[2]{0:T(128)S(1)}, u32[]{:S(2)}) copy-start(s32[2]{0:T(128)S(1)} %get-tuple-element.276) | copy-start | bytes 28 | tf_op jit(solution)/shard_map/while
  77.9 7.9 %copy-start.3 = (f32[128,8,128]{0,2,1:T(8,128)S(1)}, f32[128,8,128]{0,2,1:T(8,128)}, u32[]{:S(2)}) copy-start(f32[128,8,128]{0,2,1:T(8,128)} %get-tuple-element.261) | copy-start | bytes 1572868 | tf_op jit(solution)/shard_map/while
  83.0 3.4 %copy-start.2 = (f32[128,8,1024]{0,2,1:T(8,128)S(1)}, f32[128,8,1024]{0,2,1:T(8,128)}, u32[]{:S(2)}) copy-start(f32[128,8,1024]{0,2,1:T(8,128)} %get-tuple-element.240) | copy-start | bytes 12582916 | tf_op jit(solution)/shard_map/while
  86.4 2.1 copy-start.18
  87.7 0.8 copy-start.4
  88.6 5.2 %copy-start.17 = (s32[2]{0:T(128)}, s32[2]{0:T(128)S(1)}, u32[]{:S(2)}) copy-start(s32[2]{0:T(128)S(1)} %get-tuple-element.276) | copy-start | bytes 28 | tf_op jit(solution)/shard_map/while
  100.6 7.9 %copy-start.3 = (f32[128,8,128]{0,2,1:T(8,128)S(1)}, f32[128,8,128]{0,2,1:T(8,128)}, u32[]{:S(2)}) copy-start(f32[128,8,128]{0,2,1:T(8,128)} %get-tuple-element.261) | copy-start | bytes 1572868 | tf_op jit(solution)/shard_map/while
  105.6 3.4 %copy-start.2 = (f32[128,8,1024]{0,2,1:T(8,128)S(1)}, f32[128,8,1024]{0,2,1:T(8,128)}, u32[]{:S(2)}) copy-start(f32[128,8,1024]{0,2,1:T(8,128)} %get-tuple-element.240) | copy-start | bytes 12582916 | tf_op jit(solution)/shard_map/while
  109.1 2.1 copy-start.18
  110.4 0.8 copy-start.4
  111.2 5.4 %copy-start.8 = (bf16[64,2048]{1,0:T(8,128)(2,1)S(1)}, bf16[64,2048]{1,0:T(8,128)(2,1)}, u32[]{:S(2)}) copy-start(bf16[64,2048]{1,0:T(8,128)(2,1)} %param.20) | copy-start | bytes 786436
  116.7 5.1 %copy-start.14 = (f32[2048]{0:T(1024)S(1)}, f32[2048]{0:T(1024)}, u32[]{:S(2)}) copy-start(f32[2048]{0:T(1024)} %param.29) | copy-start | bytes 24580
  116.7 5.2 %copy-start.9 = (pred[64,512]{1,0:T(8,128)(4,1)S(1)}, pred[64,512]{1,0:T(8,128)(4,1)}, u32[]{:S(2)}) copy-start(pred[64,512]{1,0:T(8,128)(4,1)} %fusion.72) | copy-start | bytes 98308
  121.8 2.3 copy-start.5
  124.1 54.3 %all-to-all-start.1 = ((bf16[16,1,32,2048]{3,2,1,0:T(8,128)(2,1)}), bf16[16,1,32,2048]{3,2,1,0:T(8,128)(2,1)S(1)}, u32[]{:S(2)}, u32[]{:S(2)}) async-start(bf16[16,1,32,2048]{3,2,1,0:T(8,128)(2,1)} %bitcast.4), calls=%async_computation.1 | async-start | bytes 4194304 | tf_op jit(solution)/shard_map/all_to_all | solution.py:201
  130.0 52.2 %all-gather.9.cloned.1.call-start = ((), (), s32[]{:S(2)}) async-start(), calls=%async_computation.5 | async-start | bytes 3145728 | tf_op jit(solution)/shard_map/all_gather | solution.py:128
  130.7 54.7 %all-gather.11.cloned.1.call-start = ((), (), s32[]{:S(2)}) async-start(), calls=%async_computation.6 | async-start | bytes 3145728 | tf_op jit(solution)/shard_map/all_gather | solution.py:129
  185.4 2.1 copy-start.7
  189.5 5.2 %copy-start.16 = (f32[64,4]{0,1:T(4,128)S(1)}, f32[64,4]{0,1:T(4,128)}, u32[]{:S(2)}) copy-start(f32[64,4]{0,1:T(4,128)} %param.31) | copy-start | bytes 3076
  189.5 5.2 %copy-start.12 = (s32[64,4]{0,1:T(4,128)S(1)}, s32[64,4]{0,1:T(4,128)}, u32[]{:S(2)}) copy-start(s32[64,4]{0,1:T(4,128)} %copy-done.11) | copy-start | bytes 3076
  189.5 6.0 %copy-start.6 = (bf16[2048,512]{1,0:T(8,128)(2,1)S(1)}, bf16[2048,512]{1,0:T(8,128)(2,1)}, u32[]{:S(2)}) copy-start(bf16[2048,512]{1,0:T(8,128)(2,1)} %param.35) | copy-start | bytes 6291460
  189.5 53.0 %all-to-all-start.2 = ((bf16[16,1,32,2048]{3,2,1,0:T(8,128)(2,1)}), bf16[16,1,32,2048]{3,2,1,0:T(8,128)(2,1)}, u32[]{:S(2)}, u32[]{:S(2)}) async-start(bf16[16,1,32,2048]{3,2,1,0:T(8,128)(2,1)} %fusion.40), calls=%async_computation.2 | async-start | bytes 4194304 | tf_op jit(solution)/shard_map/all_to_all | solution.py:219
  242.6 7.1 %copy-start.1 = (bf16[512,3072]{1,0:T(8,128)(2,1)S(1)}, bf16[512,3072]{1,0:T(8,128)(2,1)}, u32[]{:S(2)}) copy-start(bf16[512,3072]{1,0:T(8,128)(2,1)} %param.26) | copy-start | bytes 9437188
Sparse Core Ops, SparseCore 0:
  10.1 55.6 all-gather.4
  67.4 10.2 all-gather.6
  132.3 11.2 all-gather.8
  145.0 11.7 all-gather.10
where the time goes:
time: 257 us; the launch traced here: 256 us
  waiting for transfers between devices  108 us (42%)
  matrix products  51.4 us (20%)
  blocking collectives  39.1 us (15%)
  other arithmetic  17.4 us (7%)
  local copies, waits for them, and re-layouts  13.6 us (5%)
  between operations  13.4 us (5%)
  starting transfers between devices  11.2 us (4%)
    all_to_all x1, waiting for transfers between devices, shards(): lax.all_to_all(outgoing, 'sp', split_axis=0, concat_axis=0, tiled=True)  47 us
    all_to_all x1, waiting for transfers between devices, shards(): lax.all_to_all(summed, 'sp', split_axis=0, concat_axis=0, tiled=True)  46.5 us
    all_gather x1, blocking collectives, attend_all(): rot_piece = lax.all_gather(rot_shard, 'sp', axis=0, tiled=True)  35.2 us
    all_gather x1, waiting for transfers between devices, attend_all(): lat_piece = lax.all_gather(lat_shard, 'sp', axis=0, tiled=True)  12.2 us
    dot_general x2, matrix products, absorb(): jnp.einsum('qhr,kr->qhk', queries[:, :, KEY_PLAIN_WIDTH:], shared_rot, pr...  10 us
    while x26, local copies, waits for them, and re-layouts  6.17 us
    all_to_all x1, starting transfers between devices, shards(): lax.all_to_all(outgoing, 'sp', split_axis=0, concat_axis=0, tiled=True)  5.91 us
    reduce_sum x2, other arithmetic, absorb(): new_sum = run_sum * factor + jnp.sum(weights, axis=-1)  5.81 us
  transfers between devices with their start and end apart: 6, of which 3 were waited for; matrix products, arithmetic and copies ran while one was open for 27% of the time, Pallas kernels for 0%

commit v1 on v0

--- a/solution.py
+++ b/solution.py
@@ -9,6 +9,22 @@
 epsilon = 1e-06
 routed_scale = 2.5
 theta_base = 10000.0
+
+
+def collect(x, axis, dim):
+    ways, here, turn = (lax.axis_size(axis), lax.axis_index(axis), x.shape[dim])
+    dims = [n * ways if d == dim else n for d, n in enumerate(x.shape)]
+    full = lax.dynamic_update_slice_in_dim(jnp.zeros(dims, x.dtype), x, here * turn, axis=dim)
+    going_up = going_down = x
+    for far in range(1, ways // 2 + 1):
+        going_up = lax.ppermute(going_up, axis, [(d, (d + 1) % ways) for d in range(ways)])
+        full = lax.dynamic_update_slice_in_dim(full, going_up, (here - far) % ways * turn, axis=dim)
+        if 2 * far < ways:
+            going_down = lax.ppermute(going_down, axis, [(d, (d - 1) % ways) for d in range(ways)])
+            full = lax.dynamic_update_slice_in_dim(
+                full, going_down, (here + far) % ways * turn, axis=dim
+            )
+    return full
 
 
 def rms_scale(values, scales):
@@ -86,7 +102,7 @@
         jnp.zeros((query_rows, head_count, VALUE_HEAD_WIDTH), jnp.float32),
     )
     lat_piece = lax.all_gather(lat_shard, "sp", axis=0, tiled=True)
-    rot_piece = lax.all_gather(rot_shard, "sp", axis=0, tiled=True)
+    rot_piece = collect(rot_shard, "sp", 0)
     span_rows = key_span(lat_piece.shape[0])
     block_total = lat_piece.shape[0] // span_rows
 

time: 257 us -> 267 us (1.039)
  starting transfers between devices: 11.2 us -> 46.8 us
  blocking collectives: 39.1 us -> 3.94 us
  local copies, waits for them, and re-layouts: 13.6 us -> 24.2 us
    all_gather x1 -> x0, blocking collectives: 35.2 us -> none  [attend_all(): rot_piece = lax.all_gather(rot_shard, 'sp', axis=0, tiled=True)]
    ppermute x0 -> x15, starting transfers between devices: none -> 26.3 us  [the longest x8 19.7 us: collect(): lax.ppermute(going_up, axis, [(d, (d + 1) % ways) for d in range(ways)])]
    dynamic_update_slice x0 -> x16, local copies, waits for them, and re-layouts: none -> 9.7 us  [the longest x8 4.85 us: collect(): lax.dynamic_update_slice_in_dim(full, going_up, (here - far) % ways * tur...]
    all_to_all x1, starting transfers between devices: 5.91 us -> 14.8 us  [shards(): lax.all_to_all(outgoing, 'sp', split_axis=0, concat_axis=0, tiled=True)]
    all_gather x1, waiting for transfers between devices: 12.2 us -> 7.93 us  [attend_all(): lat_piece = lax.all_gather(lat_shard, 'sp', axis=0, tiled=True)]
    ppermute x0 -> x15, waiting for transfers between devices: none -> 3.64 us  [the longest x7 1.98 us: collect(): lax.ppermute(going_down, axis, [(d, (d - 1) % ways) for d in range(ways)])]
  transfers between devices with their start and end apart: 6 -> 21, of which waited for: 3 -> 12; matrix products, arithmetic and copies ran while one was open for 27% -> 30% of each run, Pallas kernels for 0% -> 0%
where the time goes in v1:
time: 267 us; the launch traced here: 266 us
  waiting for transfers between devices  107 us (40%)
  matrix products  51.3 us (19%)
  starting transfers between devices  46.8 us (18%)
  local copies, waits for them, and re-layouts  24.2 us (9%)
  other arithmetic  17.5 us (7%)
  between operations  13.5 us (5%)
  blocking collectives  3.94 us (1%)
    all_to_all x1, waiting for transfers between devices, shards(): lax.all_to_all(outgoing, 'sp', split_axis=0, concat_axis=0, tiled=True)  47.2 us
    all_to_all x1, waiting for transfers between devices, shards(): lax.all_to_all(summed, 'sp', split_axis=0, concat_axis=0, tiled=True)  46.7 us
    ppermute x8, starting transfers between devices, collect(): lax.ppermute(going_up, axis, [(d, (d + 1) % ways) for d in range(ways)])  19.7 us
    all_to_all x1, starting transfers between devices, shards(): lax.all_to_all(outgoing, 'sp', split_axis=0, concat_axis=0, tiled=True)  14.8 us
    dot_general x2, matrix products, absorb(): jnp.einsum('qhr,kr->qhk', queries[:, :, KEY_PLAIN_WIDTH:], shared_rot, pr...  9.99 us
    all_gather x1, waiting for transfers between devices, attend_all(): lat_piece = lax.all_gather(lat_shard, 'sp', axis=0, tiled=True)  7.93 us
    ppermute x7, starting transfers between devices, collect(): lax.ppermute(going_down, axis, [(d, (d - 1) % ways) for d in range(ways)])  6.58 us
    while x26, local copies, waits for them, and re-layouts  6.21 us
  transfers between devices with their start and end apart: 21, of which 12 were waited for; matrix products, arithmetic and copies ran while one was open for 30% of the time, Pallas kernels for 0%

profile of v1, /device:TPU:12, one launch (start us, length us, event | category | flops | bytes accessed | tf_op | source)
XLA Modules:
  0.0 266.2 jit_solution(5440240893028061653)
XLA Ops:
  7.3 1.5 collective-permute-start
  8.8 1.4 collective-permute-start.1
  11.3 1.0 fusion.74
  12.4 2.2 convolution_multiply_fusion
  14.6 1.4 copy.78
  18.2 2.4 constant_dynamic-slice_fusion
  22.9 2.3 collective-permute-start.3
  28.0 1.9 collective-permute-start.5
  31.6 1.8 collective-permute-start.6
  33.7 0.9 collective-permute-start.7
  36.2 2.8 %collective-permute-start.8 = (bf16[128,64]{0,1:T(8,128)(2,1)S(1)}, bf16[128,64]{0,1:T(8,128)(2,1)S(1)}, u32[]{:S(2)}, u32[]{:S(2)}) collective-permute-start(bf16[128,64]{0,1:T(8,128)(2,1)S(1)} %collective-permute-done.6), channel_id=1, source_target_pairs={{0,2},{2,4},{4,6},{6,8},{8,10},{10,12},{12,14},{14,16},{16,18},{18... | collective-permute-start | bytes 49160 | tf_op jit(solution)/shard_map/ppermute | solution.py:20
  41.0 3.7 %collective-permute-start.10 = (bf16[128,64]{0,1:T(8,128)(2,1)S(1)}, bf16[128,64]{0,1:T(8,128)(2,1)S(1)}, u32[]{:S(2)}, u32[]{:S(2)}) collective-permute-start(bf16[128,64]{0,1:T(8,128)(2,1)S(1)} %collective-permute-done.8), channel_id=1, source_target_pairs={{0,2},{2,4},{4,6},{6,8},{8,10},{10,12},{12,14},{14,16},{16,18},{18... | collective-permute-start | bytes 49160 | tf_op jit(solution)/shard_map/ppermute | solution.py:20
  46.2 4.2 %collective-permute-start.12 = (bf16[128,64]{0,1:T(8,128)(2,1)S(1)}, bf16[128,64]{0,1:T(8,128)(2,1)S(1)}, u32[]{:S(2)}, u32[]{:S(2)}) collective-permute-start(bf16[128,64]{0,1:T(8,128)(2,1)S(1)} %collective-permute-done.10), channel_id=1, source_target_pairs={{0,2},{2,4},{4,6},{6,8},{8,10},{10,12},{12,14},{14,16},{16,18},{18... | collective-permute-start | bytes 49160 | tf_op jit(solution)/shard_map/ppermute | solution.py:20
  51.9 4.4 %collective-permute-start.14 = (bf16[128,64]{0,1:T(8,128)(2,1)S(1)}, bf16[128,64]{0,1:T(8,128)(2,1)S(1)}, u32[]{:S(2)}, u32[]{:S(2)}) collective-permute-start(bf16[128,64]{0,1:T(8,128)(2,1)S(1)} %collective-permute-done.12), channel_id=1, source_target_pairs={{0,2},{2,4},{4,6},{6,8},{8,10},{10,12},{12,14},{14,16},{16,18},{18... | collective-permute-start | bytes 49160 | tf_op jit(solution)/shard_map/ppermute | solution.py:20
  58.3 7.9 %all-gather.5.cloned.1.call-done = bf16[2048,256]{1,0:T(8,128)(2,1)} async-done(((bf16[128,256]{1,0:T(8,128)(2,1)}), bf16[2048,256]{1,0:T(8,128)(2,1)}) %all-gather.5.cloned.1.call-update) | async-done | bytes 1048592 | tf_op jit(solution)/shard_map/all_gather | solution.py:104
  66.3 45.4 %while.15 = (s32[]{:T(128)}, f32[128,8]{0,1:T(8,128)S(1)}, f32[128,8]{0,1:T(8,128)S(1)}, f32[128,8,128]{0,2,1:T(8,128)}, s32[2]{0:T(128)S(1)}, /*index=5*/bf16[2...) while((s32[]{:T(128)}, f32[128,8]{0,1:T(8,128)S(1)}, ...), condition=%wide.region_5.6_spmd.clone, body=%wide.region_1.5_spmd.clone.sunk | while | flops 1756078208 | bytes 72443560 | solution.py:118
  67.5 1.3 fusion.130
  68.8 2.7 %convolution_convert_fusion.5 = bf16[1024,2048]{1,0:T(8,128)(2,1)S(1)} fusion(bf16[256,2048]{1,0:T(8,128)(2,1)} %get-tuple-element.279, f32[256]{0:T(256)S(1)} %get-tuple-element.278, f32[1024]{0:T(1024)S(1)} %add_rsqrt_fusion.4, bf16[2048,256]{1,0:T(8,128)(2,1)} %get-tuple-element.277, s32[]{:T(128)S(6)} %select_n.164), kind=kOutput, calls=%fused_computation.2.clone.1 | convolution fusion | flops 1076887552 | bytes 5772292 | tf_op jit(solution)/shard_map/while/body/eval_jaxpr/dot_general | solution.py:62
  71.5 1.5 copy.110
  73.3 2.7 fusion.132
  75.9 0.9 dynamic-slice_convert_fusion.2
  76.9 1.2 fusion.129
  78.4 5.0 %fusion.133 = (f32[128,8]{0,1:T(8,128)S(1)}, f32[128,8,1024]{0,2,1:T(8,128)}) fusion(bf16[128,8,192]{0,2,1:T(8,128)(2,1)S(1)} %copy.109, bf16[1024,32]{0,1:T(8,128)(2,1)} %get-tuple-element.236, bf16[1024,32]{0,1:T(8,128)(2,1)} %get-tuple-element.237, f32[8,1024,128]{2,1,0:T(8,128)} %fusion.132), kind=kOutput, calls=%fused_computation.137.clone.1 | convolution fusion | flops 136576000 | bytes 8654848 | tf_op jit(solution)/shard_map/while/body/eval_jaxpr/qhr,kr->qhk/dot_general | solution.py:79
  83.4 2.9 %fusion.134 = f32[128,8]{0,1:T(8,128)S(1)} fusion(f32[128,8,1024]{0,2,1:T(8,128)} %get-tuple-element.240, f32[128,8]{0,1:T(8,128)S(1)} %select_maximum_fusion.2), kind=kLoop, calls=%fused_computation.4.clone.1 | loop fusion | flops 2096128 | bytes 4202496 | tf_op jit(solution)/shard_map/while/body/eval_jaxpr/reduce_sum | solution.py:88
  86.8 1.3 fusion.136
  90.2 1.3 fusion.130
  91.5 2.7 %convolution_convert_fusion.5 = bf16[1024,2048]{1,0:T(8,128)(2,1)S(1)} fusion(bf16[256,2048]{1,0:T(8,128)(2,1)} %get-tuple-element.279, f32[256]{0:T(256)S(1)} %get-tuple-element.278, f32[1024]{0:T(1024)S(1)} %add_rsqrt_fusion.4, bf16[2048,256]{1,0:T(8,128)(2,1)} %get-tuple-element.277, s32[]{:T(128)S(6)} %select_n.164), kind=kOutput, calls=%fused_computation.2.clone.1 | convolution fusion | flops 1076887552 | bytes 5772292 | tf_op jit(solution)/shard_map/while/body/eval_jaxpr/dot_general | solution.py:62
  94.2 1.5 copy.110
  96.0 2.7 fusion.132
  98.6 0.9 dynamic-slice_convert_fusion.2
  99.6 1.2 fusion.129
  101.1 5.0 %fusion.133 = (f32[128,8]{0,1:T(8,128)S(1)}, f32[128,8,1024]{0,2,1:T(8,128)}) fusion(bf16[128,8,192]{0,2,1:T(8,128)(2,1)S(1)} %copy.109, bf16[1024,32]{0,1:T(8,128)(2,1)} %get-tuple-element.236, bf16[1024,32]{0,1:T(8,128)(2,1)} %get-tuple-element.237, f32[8,1024,128]{2,1,0:T(8,128)} %fusion.132), kind=kOutput, calls=%fused_computation.137.clone.1 | convolution fusion | flops 136576000 | bytes 8654848 | tf_op jit(solution)/shard_map/while/body/eval_jaxpr/qhr,kr->qhk/dot_general | solution.py:79
  106.1 2.9 %fusion.134 = f32[128,8]{0,1:T(8,128)S(1)} fusion(f32[128,8,1024]{0,2,1:T(8,128)} %get-tuple-element.240, f32[128,8]{0,1:T(8,128)S(1)} %select_maximum_fusion.2), kind=kLoop, calls=%fused_computation.4.clone.1 | loop fusion | flops 2096128 | bytes 4202496 | tf_op jit(solution)/shard_map/while/body/eval_jaxpr/reduce_sum | solution.py:88
  109.5 1.3 fusion.136
  111.7 1.1 divide_convert_fusion
  113.2 3.9 %all_to_all.29 = bf16[2,64,1024]{2,1,0:T(8,128)(2,1)S(1)} all-to-all(bf16[2,64,1024]{2,1,0:T(8,128)(2,1)S(1)} %all_to_all.20), channel_id=1, replica_groups=mesh['sp'=16,'tp'=2] {'tp'}, dimensions={0} | all-to-all | bytes 524288 | tf_op jit(solution)/shard_map/all_to_all | solution.py:189
  117.2 5.1 %multiply_reduce_fusion = (f32[64]{0:T(128)S(1)}, f32[64,2048]{1,0:T(8,128)S(1)}) fusion(bf16[64,2048]{1,0:T(8,128)(2,1)S(1)} %bitcast.138, bf16[2048,2048]{1,0:T(8,128)(2,1)} %param.28, bf16[64,2048]{1,0:T(8,128)(2,1)S(1)} %copy-done.8), kind=kOutput, calls=%fused_computation.75 | convolution fusion | flops 537657280 | bytes 9437440 | tf_op jit(solution)/shard_map/dot_general | solution.py:190
  122.4 2.1 convolution_convert_fusion.3
  124.5 14.8 %all-to-all-start.1 = ((bf16[16,1,32,2048]{3,2,1,0:T(8,128)(2,1)}), bf16[16,1,32,2048]{3,2,1,0:T(8,128)(2,1)S(1)}, u32[]{:S(2)}, u32[]{:S(2)}) async-start(bf16[16,1,32,2048]{3,2,1,0:T(8,128)(2,1)} %bitcast.4), calls=%async_computation.1 | async-start | bytes 4194304 | tf_op jit(solution)/shard_map/all_to_all | solution.py:217
  140.7 47.2 %all-to-all-done.1 = bf16[16,1,32,2048]{3,2,1,0:T(8,128)(2,1)S(1)} async-done(((bf16[16,1,32,2048]{3,2,1,0:T(8,128)(2,1)}), bf16[16,1,32,2048]{3,2,1,0:T(8,128)(2,1)S(1)}, u32[]{:S(2)}, u32[]{:S(2)}) %all-to-all-start.1) | async-done | bytes 2097184 | tf_op jit(solution)/shard_map/all_to_all | solution.py:217
  187.9 3.8 %fusion.51 = f32[16,1,32,512]{3,2,0,1:T(8,128)} fusion(bf16[1,2048,512]{2,1,0:T(8,128)(2,1)} %all-gather.7.cloned.1.call-done, bf16[16,1,32,2048]{3,2,1,0:T(8,128)(2,1)S(1)} %all-to-all-done.1), kind=kOutput, calls=%fused_computation.65 | convolution fusion | flops 1073741824 | bytes 5242880 | tf_op jit(solution)/shard_map/secd,edf->secf/dot_general | solution.py:218
  191.7 3.2 %fusion.66 = bf16[16,1,32,512]{3,2,0,1:T(8,128)(2,1)S(1)} fusion(bf16[1,2048,512]{2,1,0:T(8,128)(2,1)} %all-gather.9.cloned.1.call-done, bf16[16,1,32,2048]{3,2,1,0:T(8,128)(2,1)S(1)} %all-to-all-done.1, f32[16,1,32,512]{3,2,0,1:T(8,128)} %fusion.51), kind=kOutput, calls=%fused_computation.68 | convolution fusion | flops 1075314688 | bytes 5767168 | tf_op jit(solution)/shard_map/secd,edf->secf/dot_general | solution.py:219
  195.0 2.1 convolution_convert_fusion.1
  197.1 2.0 fusion.40
  199.1 5.6 %all-to-all-start.2 = ((bf16[16,1,32,2048]{3,2,1,0:T(8,128)(2,1)}), bf16[16,1,32,2048]{3,2,1,0:T(8,128)(2,1)}, u32[]{:S(2)}, u32[]{:S(2)}) async-start(bf16[16,1,32,2048]{3,2,1,0:T(8,128)(2,1)} %fusion.40), calls=%async_computation.2 | async-start | bytes 4194304 | tf_op jit(solution)/shard_map/all_to_all | solution.py:235
  206.0 46.7 %all-to-all-done.2 = bf16[16,1,32,2048]{3,2,1,0:T(8,128)(2,1)} async-done(((bf16[16,1,32,2048]{3,2,1,0:T(8,128)(2,1)}), bf16[16,1,32,2048]{3,2,1,0:T(8,128)(2,1)}, u32[]{:S(2)}, u32[]{:S(2)}) %all-to-all-start.2) | async-done | bytes 2097184 | tf_op jit(solution)/shard_map/all_to_all | solution.py:235
  252.7 3.1 %convolution_add_fusion.1 = f32[64,2048]{1,0:T(8,128)} fusion(f32[64,2048]{1,0:T(8,128)} %copy-done.5, bf16[64,512]{1,0:T(8,128)(2,1)} %fusion.77, bf16[512,2048]{1,0:T(8,128)(2,1)} %bitcast.28), kind=kOutput, calls=%fused_computation.53 | convolution fusion | flops 134348800 | bytes 3211264 | tf_op jit(solution)/shard_map/dot_general | solution.py:236
  255.8 3.9 %fusion.43 = bf16[64,2048]{1,0:T(8,128)(2,1)} fusion(f32[64,2048]{1,0:T(8,128)} %convolution_add_fusion.1, bf16[512,2048]{1,0:T(8,128)(2,1)} %param.37, bf16[64,2048]{1,0:T(8,128)(2,1)S(1)} %multiply_convert_fusion, bf16[2048,512]{1,0:T(8,128)(2,1)} %param.36, f32[64,512]{1,0:T(8,128)S(1)} %fusion.96), kind=kOutput, calls=%fused_computation.57 | convolution fusion | flops 268894208 | bytes 5373952 | tf_op jit(solution)/shard_map/dot_general | solution.py:245
  (148 shorter events, 27.7 us)
Async XLA Ops:
  6.5 5.8 %copy-start = (bf16[512,3072]{1,0:T(8,128)(2,1)S(1)}, bf16[512,3072]{1,0:T(8,128)(2,1)}, u32[]{:S(2)}) copy-start(bf16[512,3072]{1,0:T(8,128)(2,1)} %param.26) | copy-start | bytes 9437188
  6.5 59.7 %all-gather.5.cloned.1.call-start = ((), (), s32[]{:S(2)}) async-start(), calls=%async_computation.3 | async-start | bytes 1114112 | tf_op jit(solution)/shard_map/all_gather | solution.py:104
  7.3 133.4 %all-gather.7.cloned.1.call-start = ((), (), s32[]{:S(2)}) async-start(), calls=%async_computation.4 | async-start | bytes 3145728 | tf_op jit(solution)/shard_map/all_gather | solution.py:143
  7.3 14.9 %collective-permute-start = (bf16[128,64]{0,1:T(8,128)(2,1)}, bf16[128,64]{0,1:T(8,128)(2,1)S(1)}, u32[]{:S(2)}, u32[]{:S(2)}) collective-permute-start(bf16[128,64]{0,1:T(8,128)(2,1)} %param.23), channel_id=1, source_target_pairs={{0,2},{2,4},{4,6},{6,8},{8,10},{10,12},{12,14},{14,16},{16,18},{18... | collective-permute-start | bytes 49160 | tf_op jit(solution)/shard_map/ppermute | solution.py:20
  8.8 14.0 %collective-permute-start.1 = (bf16[128,64]{0,1:T(8,128)(2,1)}, bf16[128,64]{0,1:T(8,128)(2,1)S(1)}, u32[]{:S(2)}, u32[]{:S(2)}) collective-permute-start(bf16[128,64]{0,1:T(8,128)(2,1)} %param.23), channel_id=1, source_target_pairs={{0,30},{2,0},{4,2},{6,4},{8,6},{10,8},{12,10},{14,12},{16,14},{18,... | collective-permute-start | bytes 49160 | tf_op jit(solution)/shard_map/ppermute | solution.py:23
  12.4 4.8 %copy-start.15 = (s32[64,4]{0,1:T(4,128)S(1)}, s32[64,4]{0,1:T(4,128)}, u32[]{:S(2)}) copy-start(s32[64,4]{0,1:T(4,128)} %param.30) | copy-start | bytes 3076
  16.0 5.3 %copy-start.13 = (bf16[128,64]{0,1:T(8,128)(2,1)S(1)}, bf16[128,64]{0,1:T(8,128)(2,1)}, u32[]{:S(2)}) copy-start(bf16[128,64]{0,1:T(8,128)(2,1)} %param.23) | copy-start | bytes 49156
  17.2 0.8 copy-start.11
  18.2 48.1 %copy-start.10 = (f32[256]{0:T(256)S(1)}, f32[256]{0:T(256)}, u32[]{:S(2)}) copy-start(f32[256]{0:T(256)} %param.25) | copy-start | bytes 3076
  22.3 4.7 %collective-permute-start.2 = (bf16[128,64]{0,1:T(8,128)(2,1)S(1)}, bf16[128,64]{0,1:T(8,128)(2,1)S(1)}, u32[]{:S(2)}, u32[]{:S(2)}) collective-permute-start(bf16[128,64]{0,1:T(8,128)(2,1)S(1)} %collective-permute-done), channel_id=1, source_target_pairs={{0,2},{2,4},{4,6},{6,8},{8,10},{10,12},{12,14},{14,16},{16,18},{18... | collective-permute-start | bytes 49160 | tf_op jit(solution)/shard_map/ppermute | solution.py:20
  22.9 5.1 %collective-permute-start.3 = (bf16[128,64]{0,1:T(8,128)(2,1)S(1)}, bf16[128,64]{0,1:T(8,128)(2,1)S(1)}, u32[]{:S(2)}, u32[]{:S(2)}) collective-permute-start(bf16[128,64]{0,1:T(8,128)(2,1)S(1)} %collective-permute-done.1), channel_id=1, source_target_pairs={{0,30},{2,0},{4,2},{6,4},{8,6},{10,8},{12,10},{14,12},{16,14},{18,... | collective-permute-start | bytes 49160 | tf_op jit(solution)/shard_map/ppermute | solution.py:23
  26.9 4.6 %collective-permute-start.4 = (bf16[128,64]{0,1:T(8,128)(2,1)S(1)}, bf16[128,64]{0,1:T(8,128)(2,1)S(1)}, u32[]{:S(2)}, u32[]{:S(2)}) collective-permute-start(bf16[128,64]{0,1:T(8,128)(2,1)S(1)} %collective-permute-done.2), channel_id=1, source_target_pairs={{0,2},{2,4},{4,6},{6,8},{8,10},{10,12},{12,14},{14,16},{16,18},{18... | collective-permute-start | bytes 49160 | tf_op jit(solution)/shard_map/ppermute | solution.py:20
  28.0 5.7 %collective-permute-start.5 = (bf16[128,64]{0,1:T(8,128)(2,1)S(1)}, bf16[128,64]{0,1:T(8,128)(2,1)S(1)}, u32[]{:S(2)}, u32[]{:S(2)}) collective-permute-start(bf16[128,64]{0,1:T(8,128)(2,1)S(1)} %collective-permute-done.3), channel_id=1, source_target_pairs={{0,30},{2,0},{4,2},{6,4},{8,6},{10,8},{12,10},{14,12},{16,14},{18,... | collective-permute-start | bytes 49160 | tf_op jit(solution)/shard_map/ppermute | solution.py:23
  31.6 4.6 %collective-permute-start.6 = (bf16[128,64]{0,1:T(8,128)(2,1)S(1)}, bf16[128,64]{0,1:T(8,128)(2,1)S(1)}, u32[]{:S(2)}, u32[]{:S(2)}) collective-permute-start(bf16[128,64]{0,1:T(8,128)(2,1)S(1)} %collective-permute-done.4), channel_id=1, source_target_pairs={{0,2},{2,4},{4,6},{6,8},{8,10},{10,12},{12,14},{14,16},{16,18},{18... | collective-permute-start | bytes 49160 | tf_op jit(solution)/shard_map/ppermute | solution.py:20
  33.7 6.1 %collective-permute-start.7 = (bf16[128,64]{0,1:T(8,128)(2,1)S(1)}, bf16[128,64]{0,1:T(8,128)(2,1)S(1)}, u32[]{:S(2)}, u32[]{:S(2)}) collective-permute-start(bf16[128,64]{0,1:T(8,128)(2,1)S(1)} %collective-permute-done.5), channel_id=1, source_target_pairs={{0,30},{2,0},{4,2},{6,4},{8,6},{10,8},{12,10},{14,12},{16,14},{18,... | collective-permute-start | bytes 49160 | tf_op jit(solution)/shard_map/ppermute | solution.py:23
  36.2 4.7 %collective-permute-start.8 = (bf16[128,64]{0,1:T(8,128)(2,1)S(1)}, bf16[128,64]{0,1:T(8,128)(2,1)S(1)}, u32[]{:S(2)}, u32[]{:S(2)}) collective-permute-start(bf16[128,64]{0,1:T(8,128)(2,1)S(1)} %collective-permute-done.6), channel_id=1, source_target_pairs={{0,2},{2,4},{4,6},{6,8},{8,10},{10,12},{12,14},{14,16},{16,18},{18... | collective-permute-start | bytes 49160 | tf_op jit(solution)/shard_map/ppermute | solution.py:20
  39.7 5.2 %collective-permute-start.9 = (bf16[128,64]{0,1:T(8,128)(2,1)S(1)}, bf16[128,64]{0,1:T(8,128)(2,1)S(1)}, u32[]{:S(2)}, u32[]{:S(2)}) collective-permute-start(bf16[128,64]{0,1:T(8,128)(2,1)S(1)} %collective-permute-done.7), channel_id=1, source_target_pairs={{0,30},{2,0},{4,2},{6,4},{8,6},{10,8},{12,10},{14,12},{16,14},{18,... | collective-permute-start | bytes 49160 | tf_op jit(solution)/shard_map/ppermute | solution.py:23
  41.0 5.2 %collective-permute-start.10 = (bf16[128,64]{0,1:T(8,128)(2,1)S(1)}, bf16[128,64]{0,1:T(8,128)(2,1)S(1)}, u32[]{:S(2)}, u32[]{:S(2)}) collective-permute-start(bf16[128,64]{0,1:T(8,128)(2,1)S(1)} %collective-permute-done.8), channel_id=1, source_target_pairs={{0,2},{2,4},{4,6},{6,8},{8,10},{10,12},{12,14},{14,16},{16,18},{18... | collective-permute-start | bytes 49160 | tf_op jit(solution)/shard_map/ppermute | solution.py:20
  45.0 5.7 %collective-permute-start.11 = (bf16[128,64]{0,1:T(8,128)(2,1)S(1)}, bf16[128,64]{0,1:T(8,128)(2,1)S(1)}, u32[]{:S(2)}, u32[]{:S(2)}) collective-permute-start(bf16[128,64]{0,1:T(8,128)(2,1)S(1)} %collective-permute-done.9), channel_id=1, source_target_pairs={{0,30},{2,0},{4,2},{6,4},{8,6},{10,8},{12,10},{14,12},{16,14},{18,... | collective-permute-start | bytes 49160 | tf_op jit(solution)/shard_map/ppermute | solution.py:23
  46.2 5.7 %collective-permute-start.12 = (bf16[128,64]{0,1:T(8,128)(2,1)S(1)}, bf16[128,64]{0,1:T(8,128)(2,1)S(1)}, u32[]{:S(2)}, u32[]{:S(2)}) collective-permute-start(bf16[128,64]{0,1:T(8,128)(2,1)S(1)} %collective-permute-done.10), channel_id=1, source_target_pairs={{0,2},{2,4},{4,6},{6,8},{8,10},{10,12},{12,14},{14,16},{16,18},{18... | collective-permute-start | bytes 49160 | tf_op jit(solution)/shard_map/ppermute | solution.py:20
  50.7 6.2 %collective-permute-start.13 = (bf16[128,64]{0,1:T(8,128)(2,1)S(1)}, bf16[128,64]{0,1:T(8,128)(2,1)S(1)}, u32[]{:S(2)}, u32[]{:S(2)}) collective-permute-start(bf16[128,64]{0,1:T(8,128)(2,1)S(1)} %collective-permute-done.11), channel_id=1, source_target_pairs={{0,30},{2,0},{4,2},{6,4},{8,6},{10,8},{12,10},{14,12},{16,14},{18,... | collective-permute-start | bytes 49160 | tf_op jit(solution)/shard_map/ppermute | solution.py:23
  51.9 5.9 %collective-permute-start.14 = (bf16[128,64]{0,1:T(8,128)(2,1)S(1)}, bf16[128,64]{0,1:T(8,128)(2,1)S(1)}, u32[]{:S(2)}, u32[]{:S(2)}) collective-permute-start(bf16[128,64]{0,1:T(8,128)(2,1)S(1)} %collective-permute-done.12), channel_id=1, source_target_pairs={{0,2},{2,4},{4,6},{6,8},{8,10},{10,12},{12,14},{14,16},{16,18},{18... | collective-permute-start | bytes 49160 | tf_op jit(solution)/shard_map/ppermute | solution.py:20
  66.3 5.2 %copy-start.17 = (s32[2]{0:T(128)}, s32[2]{0:T(128)S(1)}, u32[]{:S(2)}) copy-start(s32[2]{0:T(128)S(1)} %get-tuple-element.276) | copy-start | bytes 28 | tf_op jit(solution)/shard_map/while
  78.4 7.9 %copy-start.3 = (f32[128,8,128]{0,2,1:T(8,128)S(1)}, f32[128,8,128]{0,2,1:T(8,128)}, u32[]{:S(2)}) copy-start(f32[128,8,128]{0,2,1:T(8,128)} %get-tuple-element.261) | copy-start | bytes 1572868 | tf_op jit(solution)/shard_map/while
  83.4 3.4 %copy-start.2 = (f32[128,8,1024]{0,2,1:T(8,128)S(1)}, f32[128,8,1024]{0,2,1:T(8,128)}, u32[]{:S(2)}) copy-start(f32[128,8,1024]{0,2,1:T(8,128)} %get-tuple-element.240) | copy-start | bytes 12582916 | tf_op jit(solution)/shard_map/while
  86.8 2.2 copy-start.18
  88.1 0.9 copy-start.4
  89.0 5.2 %copy-start.17 = (s32[2]{0:T(128)}, s32[2]{0:T(128)S(1)}, u32[]{:S(2)}) copy-start(s32[2]{0:T(128)S(1)} %get-tuple-element.276) | copy-start | bytes 28 | tf_op jit(solution)/shard_map/while
  101.1 7.9 %copy-start.3 = (f32[128,8,128]{0,2,1:T(8,128)S(1)}, f32[128,8,128]{0,2,1:T(8,128)}, u32[]{:S(2)}) copy-start(f32[128,8,128]{0,2,1:T(8,128)} %get-tuple-element.261) | copy-start | bytes 1572868 | tf_op jit(solution)/shard_map/while
  106.1 3.4 %copy-start.2 = (f32[128,8,1024]{0,2,1:T(8,128)S(1)}, f32[128,8,1024]{0,2,1:T(8,128)}, u32[]{:S(2)}) copy-start(f32[128,8,1024]{0,2,1:T(8,128)} %get-tuple-element.240) | copy-start | bytes 12582916 | tf_op jit(solution)/shard_map/while
  109.5 2.2 copy-start.18
  110.9 0.9 copy-start.4
  111.7 5.4 %copy-start.8 = (bf16[64,2048]{1,0:T(8,128)(2,1)S(1)}, bf16[64,2048]{1,0:T(8,128)(2,1)}, u32[]{:S(2)}) copy-start(bf16[64,2048]{1,0:T(8,128)(2,1)} %param.20) | copy-start | bytes 786436
  117.1 5.1 %copy-start.14 = (f32[2048]{0:T(1024)S(1)}, f32[2048]{0:T(1024)}, u32[]{:S(2)}) copy-start(f32[2048]{0:T(1024)} %param.29) | copy-start | bytes 24580
  117.2 5.2 %copy-start.9 = (pred[64,512]{1,0:T(8,128)(4,1)S(1)}, pred[64,512]{1,0:T(8,128)(4,1)}, u32[]{:S(2)}) copy-start(pred[64,512]{1,0:T(8,128)(4,1)} %fusion.72) | copy-start | bytes 98308
  122.3 2.3 copy-start.5
  124.5 63.4 %all-to-all-start.1 = ((bf16[16,1,32,2048]{3,2,1,0:T(8,128)(2,1)}), bf16[16,1,32,2048]{3,2,1,0:T(8,128)(2,1)S(1)}, u32[]{:S(2)}, u32[]{:S(2)}) async-start(bf16[16,1,32,2048]{3,2,1,0:T(8,128)(2,1)} %bitcast.4), calls=%async_computation.1 | async-start | bytes 4194304 | tf_op jit(solution)/shard_map/all_to_all | solution.py:217
  139.3 52.4 %all-gather.9.cloned.1.call-start = ((), (), s32[]{:S(2)}) async-start(), calls=%async_computation.5 | async-start | bytes 3145728 | tf_op jit(solution)/shard_map/all_gather | solution.py:144
  140.1 54.9 %all-gather.11.cloned.1.call-start = ((), (), s32[]{:S(2)}) async-start(), calls=%async_computation.6 | async-start | bytes 3145728 | tf_op jit(solution)/shard_map/all_gather | solution.py:145
  195.0 2.1 copy-start.7
  199.1 5.6 %copy-start.16 = (f32[64,4]{0,1:T(4,128)S(1)}, f32[64,4]{0,1:T(4,128)}, u32[]{:S(2)}) copy-start(f32[64,4]{0,1:T(4,128)} %param.31) | copy-start | bytes 3076
  199.1 5.6 %copy-start.12 = (s32[64,4]{0,1:T(4,128)S(1)}, s32[64,4]{0,1:T(4,128)}, u32[]{:S(2)}) copy-start(s32[64,4]{0,1:T(4,128)} %copy-done.11) | copy-start | bytes 3076
  199.1 6.4 %copy-start.6 = (bf16[2048,512]{1,0:T(8,128)(2,1)S(1)}, bf16[2048,512]{1,0:T(8,128)(2,1)}, u32[]{:S(2)}) copy-start(bf16[2048,512]{1,0:T(8,128)(2,1)} %param.35) | copy-start | bytes 6291460
  199.1 53.6 %all-to-all-start.2 = ((bf16[16,1,32,2048]{3,2,1,0:T(8,128)(2,1)}), bf16[16,1,32,2048]{3,2,1,0:T(8,128)(2,1)}, u32[]{:S(2)}, u32[]{:S(2)}) async-start(bf16[16,1,32,2048]{3,2,1,0:T(8,128)(2,1)} %fusion.40), calls=%async_computation.2 | async-start | bytes 4194304 | tf_op jit(solution)/shard_map/all_to_all | solution.py:235
  252.7 7.0 %copy-start.1 = (bf16[512,3072]{1,0:T(8,128)(2,1)S(1)}, bf16[512,3072]{1,0:T(8,128)(2,1)}, u32[]{:S(2)}) copy-start(bf16[512,3072]{1,0:T(8,128)(2,1)} %param.26) | copy-start | bytes 9437188
Sparse Core Ops, SparseCore 0:
  10.1 56.1 all-gather.4
  67.8 10.0 all-gather.6
  141.7 11.3 all-gather.8
  154.4 11.7 all-gather.10
